TPU v7x, 32 devices: a whole 2x2x4 slice. The times are simulated.
32 devices in a mesh: ep: 8 (over z, x), tp: 4 (over y, core).
Axes of the slice: x: 2, y: 2, z: 4, core: 2. Of those that a mesh axis runs over, the one named last changes fastest.
Arguments:
- queries: bfloat16 [4096, 1024], P('ep', 'tp'), may hold values from -6 to 6
- key_input: bfloat16 [4096, 256], P('ep'), may hold values from -6 to 6
- value_input: bfloat16 [4096, 256], P('ep'), may hold values from -6 to 6
- query_gain: float32 [64], replicated, may hold values from 0.1 to 1.9
- key_gain: float32 [64], replicated, may hold values from 0.1 to 1.9
- mix_out_weight: bfloat16 [1024, 2048], P('tp'), may hold values from -0.1875 to 0.1875
- expert_input: bfloat16 [1280, 2048], P('ep'), may hold values from -6 to 6
- ffn_gain: float32 [2048], replicated, may hold values from 0.1 to 1.9
- routes: int32 [1280, 2], P('ep'), may hold values from 0 to 7, all different within a row; in each aligned block of 160 rows (0 to 159, 160 to 319, ...) at most 60 rows name the same one
- route_scores: float32 [1280, 2], P('ep'), may hold values from 0.1 to 1
- gate_weight: bfloat16 [8, 2048, 4096], P('ep', None, 'tp'), may hold values from -0.125 to 0.125
- up_weight: bfloat16 [8, 2048, 4096], P('ep', None, 'tp'), may hold values from -0.125 to 0.125
- down_weight: bfloat16 [8, 4096, 2048], P('ep', 'tp'), may hold values from -0.09375 to 0.09375
Outputs:
- mixed_rows: bfloat16 [4096, 2048], P(('ep', 'tp'))
- expert_out: bfloat16 [1280, 2048], P('ep', 'tp')
Inputs may be any that keep to these rules, and one draw needn't show every extreme that they name: `routes`: each row names 2 different experts. Within the rows of one index of ep (aligned blocks of 160 rows) no expert is named by more than 60 rows, and in every draw some expert is named by exactly 60 rows of some block.
All inputs are finite; a program needn't handle non-finite values.
Results may differ from a plain program's by a relative error of at most 0.019.
The roundings to bfloat16 on the way count: a program that leaves them out, or rounds other values in their place, can miss the bound.
Values may be sent and summed in bfloat16 or wider, within the bound.
A program may use at most 64 MiB of HBM per device.

v0:
```python
import functools
import math

import jax
import jax.numpy as jnp
from jax import lax
from jax.experimental import pallas as pl
from jax.experimental.pallas import tpu as pltpu
from jax.sharding import PartitionSpec as P

HEADS = 16
KV_HEADS = 4
HD = 64
GRID_W = 64
EPSILON = 1e-06
ROPE_BASE = 10000.0
MESH = pl.DeviceIdType.MESH
LANES = 128
BF = jnp.bfloat16
F32 = jnp.float32


def prep(values, gain, cos_table, sin_table):
    width = values.shape[1]
    squares = values * values
    high = squares.astype(BF)
    low = (squares - high.astype(F32)).astype(BF)
    rows = lax.broadcasted_iota(jnp.int32, (width, width), 0) // HD
    cols = lax.broadcasted_iota(jnp.int32, (width, width), 1) // HD
    same = jnp.where(rows == cols, 1.0, 0.0).astype(BF)
    total = jnp.dot(high, same, preferred_element_type=F32) + jnp.dot(
        low, same, preferred_element_type=F32
    )
    gain = jnp.concatenate([gain] * (width // HD), axis=1)
    normed = values * lax.rsqrt(total * (1.0 / HD) + EPSILON) * gain
    lane = lax.broadcasted_iota(jnp.int32, normed.shape, 1)
    quarter = HD // 4
    partner = jnp.where(
        lane % (2 * quarter) < quarter,
        pltpu.roll(normed, width - quarter, 1),
        pltpu.roll(normed, quarter, 1),
    )
    return normed * cos_table + partner * sin_table


def angle_tables(start, rows):
    quarter = HD // 4
    many = rows // GRID_W

    def both(count, first):
        shape = (count, LANES)
        place = lax.broadcasted_iota(jnp.int32, shape, 0) + first
        lane = lax.broadcasted_iota(jnp.int32, shape, 1)
        turn = lane % quarter
        inverse = jnp.zeros(shape, F32)
        for j in range(quarter):
            inverse = jnp.where(turn == j, ROPE_BASE ** (-j / quarter), inverse)
        angle = place.astype(F32) * inverse
        sign = jnp.where(lane % (2 * quarter) < quarter, -1.0, 1.0)
        return jnp.cos(angle), jnp.sin(angle) * sign

    tables = []
    for by_row, by_col in zip(both(max(many, 8), start // GRID_W), both(GRID_W, 0)):
        lane = lax.broadcasted_iota(jnp.int32, by_col.shape, 1)
        tables.append(
            jnp.concatenate(
                [jnp.where(lane % HD < HD // 2, by_row[i:i + 1, :], by_col) for i in range(many)],
                axis=0,
            )
        )
    return tables


def kernel(
    n_ep, n_tp, heads, model_width,
    q_any, k_any, v_any, qg_ref, kg_ref, wmix_ref, x_any, gain_ref, routes_ref,
    scores_ref, wg_ref, wu_ref, wd_ref,
    mixed_ref, out_ref,
    q_ref, k_in, v_in, x_ref, kv_buf, q_buf, x_out, x_buf, scaled, hid, wg, wu, wd, wmix, dp_buf, ep_in, es_buf, ey_in,
    ret_out, ret_in, mp_out, mp_in, ms_out, my_in,
    w_sem, kv_s, kv_r, di_s, di_r, dy_s, dy_r, dc_s, dc_r, ep_s, ep_r, ey_s, ey_r, rt_s, rt_r,
    mp_s, mp_r, my_s, my_r,
):
    n_y = n_tp // 2
    me = lax.axis_index("ep")
    tp = lax.axis_index("tp")
    my_y, core = tp // 2, tp % 2
    mate = my_y * 2 + 1 - core
    rows = q_ref.shape[0]
    kv_head = tp * heads // (HEADS // KV_HEADS)
    kv_tile = pl.ds(pl.multiple_of(kv_head // 2 * LANES, LANES), LANES)
    slots_per = x_buf.shape[2]
    slots = n_ep * slots_per
    col_w = x_buf.shape[3]
    tokens = x_ref.shape[0]
    x_cols = pl.ds(pl.multiple_of(tp * col_w, col_w), col_w)

    def y_peer(j):
        return (my_y + j) % n_y

    loads = [
        pltpu.make_async_copy(src, dst, w_sem.at[i])
        for i, (src, dst) in enumerate(
            (
                (x_any.at[:, x_cols], x_ref),
                (k_any.at[:, kv_tile], k_in),
                (v_any.at[:, kv_tile], v_in),
                (q_any, q_ref),
                (wg_ref.at[0], wg),
                (wu_ref.at[0], wu),
                (wd_ref.at[0], wd),
                (wmix_ref, wmix),
            )
        )
    ]
    for load in loads:
        load.start()

    barrier = pltpu.get_barrier_semaphore()

    def greet(o, carry):
        pl.semaphore_signal(barrier, inc=1, device_id=((me + o) % n_ep, tp), device_id_type=MESH)
        return carry

    lax.fori_loop(1, n_ep, greet, 0)
    for j in range(1, n_y):
        pl.semaphore_signal(
            barrier, inc=1, device_id=(me, y_peer(j) * 2 + core), device_id_type=MESH
        )
    pl.semaphore_signal(barrier, inc=1, device_id=(me, mate), device_id_type=MESH)

    expert_row = lax.broadcasted_iota(jnp.int32, (n_ep, tokens), 0)
    first = jnp.where(expert_row == routes_ref[0:1, :], 1.0, 0.0)
    second = jnp.where(expert_row == routes_ref[1:2, :], 1.0, 0.0)
    earlier = jnp.where(
        lax.broadcasted_iota(jnp.int32, (tokens, tokens), 0)
        < lax.broadcasted_iota(jnp.int32, (tokens, tokens), 1),
        1.0,
        0.0,
    ).astype(BF)
    before = jnp.dot((first + second).astype(BF), earlier, preferred_element_type=F32)
    place = before + expert_row.astype(F32) * slots_per
    slot_a = jnp.sum(first * place, axis=0, keepdims=True).astype(jnp.int32)
    slot_b = jnp.sum(second * place, axis=0, keepdims=True).astype(jnp.int32)
    slot_row = lax.broadcasted_iota(jnp.int32, (slots, tokens), 0)
    pick_a = jnp.where(slot_row == slot_a, 1.0, 0.0).astype(BF)
    pick_b = jnp.where(slot_row == slot_b, 1.0, 0.0).astype(BF)
    loads[0].wait()
    sent = jnp.dot(pick_a + pick_b, x_ref[...], preferred_element_type=F32).astype(BF)
    x_out[...] = sent.reshape(x_out.shape)
    x_buf[tp, me] = x_out[me]

    pl.semaphore_wait(barrier, n_ep - 1 + n_y)

    def disp(peer):
        return pltpu.make_async_remote_copy(
            x_out.at[peer], x_buf.at[tp, me], di_s.at[peer], di_r.at[me],
            device_id=(peer, tp), device_id_type=MESH,
        )

    def disp_in(source):
        return pltpu.make_async_remote_copy(
            x_out.at[source], x_buf.at[tp, source], di_s.at[source], di_r.at[source],
            device_id=(source, tp), device_id_type=MESH,
        )

    n_x = 1 << ((n_ep.bit_length() - 1) // 2)
    n_z = n_ep // n_x
    my_z, my_x = me // n_x, me % n_x

    def z_peer(o):
        return (my_z + o) % n_z * n_x + my_x

    def x_peer(o):
        return my_z * n_x + (my_x + o) % n_x

    def kv_copy(peer, origin, leg):
        return pltpu.make_async_remote_copy(
            kv_buf.at[origin], kv_buf.at[origin], kv_s.at[leg], kv_r.at[origin],
            device_id=(peer, tp), device_id_type=MESH,
        )

    def over_y(j, source, owner):
        return pltpu.make_async_remote_copy(
            x_buf.at[owner * 2 + core, source], x_buf.at[owner * 2 + core, source],
            dy_s.at[y_peer(j), source], dy_r.at[owner, source],
            device_id=(me, y_peer(j) * 2 + core), device_id_type=MESH,
        )

    def start_disp(o, carry):
        disp((me + o) % n_ep).start()
        return carry

    lax.fori_loop(1, n_ep, start_disp, 0)
    for j in range(1, n_y):
        over_y(j, me, my_y).start()

    cos_table, sin_table = angle_tables(me * rows, rows)
    loads[1].wait()
    loads[2].wait()
    odd = kv_head % 2 == 1
    key = k_in[...].astype(F32)
    value = v_in[...].astype(F32)
    key = jnp.where(odd, pltpu.roll(key, HD, 1), key)
    value = jnp.where(odd, value, pltpu.roll(value, HD, 1))
    turned = prep(key, kg_ref[...], cos_table, sin_table)
    lane = lax.broadcasted_iota(jnp.int32, key.shape, 1)
    kv_buf[me] = jnp.where(lane < HD, turned, value).astype(BF)

    loads[3].wait()
    for tile in range(q_ref.shape[1] // LANES):
        q_tile = prep(
            q_ref[:, tile * LANES:(tile + 1) * LANES].astype(F32),
            qg_ref[...], cos_table, sin_table,
        )
        q_lane = lax.broadcasted_iota(jnp.int32, q_tile.shape, 1)
        for part in range(2):
            head = tile * 2 + part
            if head < heads:
                moved = q_tile if part == 0 else pltpu.roll(q_tile, HD, 1)
                q_buf[head] = jnp.where(q_lane < HD, moved, 0.0).astype(BF)

    def forward(o, carry):
        source = (me + n_ep - o) % n_ep
        disp_in(source).wait_recv()
        for j in range(1, n_y):
            over_y(j, source, my_y).start()
        return carry

    lax.fori_loop(1, n_ep, forward, 0)
    for o in range(1, n_x):
        kv_copy(x_peer(o), me, o).start()
    for o in range(1, n_z):
        kv_copy(z_peer(o), me, o * n_x).start()

    def to_mate(owner, mine):
        quarter = owner * 2 + mine
        return pltpu.make_async_remote_copy(
            x_buf.at[quarter], x_buf.at[quarter], dc_s.at[owner], dc_r.at[owner],
            device_id=(me, mate), device_id_type=MESH,
        )

    to_mate(my_y, core).start()
    for j in range(1, n_y):
        owner = y_peer(j)

        def arrived(source, carry):
            over_y(j, source, owner).wait_recv()
            return carry

        lax.fori_loop(0, n_ep, arrived, 0)
        to_mate(owner, core).start()
    for j in range(n_y):
        to_mate(y_peer(j), 1 - core).wait_recv()

    power = jnp.zeros((slots, 1), F32)
    for q in range(n_tp):
        x_q = x_buf[q].reshape(slots, col_w).astype(F32)
        power = power + jnp.sum(x_q * x_q, axis=1, keepdims=True)
        scaled[:, q * col_w:(q + 1) * col_w] = (
            x_q * gain_ref[:, q * col_w:(q + 1) * col_w]
        ).astype(BF)
    row_scale = lax.rsqrt(power * (1.0 / model_width) + EPSILON)
    loads[4].wait()
    loads[5].wait()
    hidden_w = wg.shape[1]
    tile_w = math.gcd(hidden_w, 256)

    def hidden_tile(i, carry):
        cols = pl.ds(pl.multiple_of(i * tile_w, tile_w), tile_w)
        gate = row_scale * jnp.dot(scaled[...], wg[:, cols], preferred_element_type=F32)
        up = row_scale * jnp.dot(scaled[...], wu[:, cols], preferred_element_type=F32)
        hid[:, cols] = (gate / (1.0 + jnp.exp(-gate)) * up).astype(BF)
        return carry

    lax.fori_loop(0, hidden_w // tile_w, hidden_tile, 0)
    loads[6].wait()
    for q in range(n_tp):
        dp_buf[q] = jnp.dot(
            hid[...], wd[:, q * col_w:(q + 1) * col_w], preferred_element_type=F32
        ).astype(BF)

    for o in range(1, n_z):
        origin = z_peer(n_z - o)
        kv_copy(origin, origin, 0).wait_recv()
        for i in range(1, n_x):
            kv_copy(x_peer(i), origin, o * n_x + i).start()

    def expert_mate(owner, side):
        return pltpu.make_async_remote_copy(
            dp_buf.at[owner * 2 + side], ep_in.at[owner], ep_s.at[owner], ep_r.at[owner],
            device_id=(me, mate), device_id_type=MESH,
        )

    def expert_y(j):
        return pltpu.make_async_remote_copy(
            es_buf.at[y_peer(j)], ey_in.at[my_y], ey_s.at[y_peer(j)], ey_r.at[my_y],
            device_id=(me, y_peer(j) * 2 + core), device_id_type=MESH,
        )

    def expert_y_in(j):
        return pltpu.make_async_remote_copy(
            es_buf.at[y_peer(j)], ey_in.at[y_peer(j)], ey_s.at[y_peer(j)], ey_r.at[y_peer(j)],
            device_id=(me, y_peer(j) * 2 + core), device_id_type=MESH,
        )

    for j in range(n_y):
        expert_mate(y_peer((j + 1) % n_y), 1 - core).start()

    def mate_sum(j):
        owner = y_peer(j)
        expert_mate(owner, core).wait_recv()
        return dp_buf[owner * 2 + core].astype(F32) + ep_in[owner].astype(F32)

    for j in range(1, n_y):
        es_buf[y_peer(j)] = mate_sum(j).astype(BF)
        expert_y(j).start()

    def ret(peer, origin):
        return pltpu.make_async_remote_copy(
            ret_out.at[peer], ret_in.at[origin], rt_s.at[peer], rt_r.at[origin],
            device_id=(peer, tp), device_id_type=MESH,
        )

    def return_rows():
        total = mate_sum(0)
        for j in range(1, n_y):
            expert_y_in(j).wait_recv()
            total = total + ey_in[y_peer(j)].astype(F32)
        ret_out[...] = total.astype(BF).reshape(ret_out.shape)
        ret_in[me] = ret_out[me]

        def start_ret(o, carry):
            ret((me + o) % n_ep, me).start()
            return carry

        lax.fori_loop(1, n_ep, start_ret, 0)

    piece = rows // n_y
    half = piece // 2
    factor = HD ** (-0.5) * math.log2(math.e)

    def mix_mate(owner, side):
        return pltpu.make_async_remote_copy(
            mp_out.at[owner, side], mp_in.at[owner], mp_s.at[owner], mp_r.at[owner],
            device_id=(me, mate), device_id_type=MESH,
        )

    def mix_y(j, origin):
        return pltpu.make_async_remote_copy(
            ms_out.at[y_peer(j)], my_in.at[origin], my_s.at[y_peer(j)], my_r.at[origin],
            device_id=(me, y_peer(j) * 2 + core), device_id_type=MESH,
        )

    def attend(owner):
        start = pl.multiple_of(owner * piece, piece)
        q_rows = q_buf[:, pl.ds(start, piece), :].reshape(heads * piece, LANES)

        def one_block(block, total):
            kv = kv_buf[block]
            logits = lax.dot_general(
                q_rows, kv, (((1,), (1,)), ((), ())), preferred_element_type=F32
            )
            weights = jnp.exp2(logits * factor).astype(BF)
            kv_lane = lax.broadcasted_iota(jnp.int32, kv.shape, 1)
            values = jnp.where(kv_lane < HD, jnp.ones_like(kv), kv)
            return total + jnp.dot(weights, values, preferred_element_type=F32)

        total = lax.fori_loop(0, n_ep, one_block, jnp.zeros((heads * piece, LANES), F32))
        ratio = (total / pltpu.roll(total, HD, 1)).reshape(heads, piece, LANES)
        out_lane = lax.broadcasted_iota(jnp.int32, (piece, LANES), 1)
        tiles = []
        for tile in range(q_ref.shape[1] // LANES):
            left = pltpu.roll(ratio[2 * tile], HD, 1)
            right = ratio[2 * tile + 1] if 2 * tile + 1 < heads else jnp.zeros_like(left)
            tiles.append(jnp.where(out_lane < HD, left, right).astype(BF))
        attended = tiles[0] if len(tiles) == 1 else jnp.concatenate(tiles, axis=1)
        part = jnp.dot(attended, wmix[...], preferred_element_type=F32).astype(BF)
        mp_out[owner] = part.reshape(2, half, part.shape[1])
        mix_mate(owner, 1 - core).start()

    def mix_sum(owner):
        mix_mate(owner, core).wait_recv()
        return mp_out[owner, core].astype(F32) + mp_in[owner].astype(F32)

    for o in range(n_z):
        for i in range(1, n_x):
            origin = (my_z + n_z - o) % n_z * n_x + (my_x + n_x - i) % n_x
            kv_copy(x_peer(i), origin, 0).wait_recv()
    loads[7].wait()
    for j in range(1, n_y):
        attend(y_peer(j))
        if j == 1:
            return_rows()
        ms_out[y_peer(j)] = mix_sum(y_peer(j)).astype(BF)
        mix_y(j, my_y).start()
    attend(my_y)

    def ret_wait(o, carry):
        source = (me + n_ep - o) % n_ep
        ret(source, source).wait_recv()
        return carry

    lax.fori_loop(1, n_ep, ret_wait, 0)
    back = ret_in[...].reshape(slots, col_w)
    share_row = scores_ref[...] / jnp.sum(scores_ref[...], axis=0, keepdims=True)
    own_token = lax.broadcasted_iota(jnp.int32, (tokens, tokens), 0) == lax.broadcasted_iota(
        jnp.int32, (tokens, tokens), 1
    )
    share_a, share_b = (
        jnp.sum(jnp.where(own_token, share_row[i:i + 1, :], 0.0), axis=1, keepdims=True)
        for i in range(2)
    )
    rows_a = lax.dot_general(
        pick_a, back, (((0,), (0,)), ((), ())), preferred_element_type=F32
    )
    rows_b = lax.dot_general(
        pick_b, back, (((0,), (0,)), ((), ())), preferred_element_type=F32
    )
    out_ref[...] = (rows_a * share_a + rows_b * share_b).astype(BF)

    total = mix_sum(my_y)
    for j in range(1, n_y):
        mix_y(j, y_peer(j)).wait_recv()
        total = total + my_in[y_peer(j)].astype(F32)
    mixed_ref[...] = total.astype(BF)

    def sends(o, carry):
        peer = (me + o) % n_ep
        disp(peer).wait_send()
        kv_copy(peer, me, o).wait_send()
        ret(peer, me).wait_send()
        return carry

    lax.fori_loop(1, n_ep, sends, 0)
    for j in range(1, n_y):

        def sent_y(source, carry):
            over_y(j, source, my_y).wait_send()
            return carry

        lax.fori_loop(0, n_ep, sent_y, 0)
        expert_y(j).wait_send()
        mix_y(j, my_y).wait_send()
    for j in range(n_y):
        to_mate(y_peer(j), core).wait_send()
        expert_mate(y_peer(j), 1 - core).wait_send()
        mix_mate(y_peer(j), 1 - core).wait_send()


def local(
    n_ep, n_tp,
    queries, key_input, value_input, query_gain, key_gain, mix_out_weight, expert_input, ffn_gain,
    routes, route_scores, gate_weight, up_weight, down_weight,
):
    rows = queries.shape[0]
    heads = queries.shape[1] // HD
    n_y = n_tp // 2
    spare = heads % 2 * HD
    if spare:
        queries = jnp.pad(queries, ((0, 0), (0, spare)))
        mix_out_weight = jnp.pad(mix_out_weight, ((0, spare), (0, 0)))
    width = expert_input.shape[1]
    col_w = width // n_tp
    tokens, top = routes.shape
    capacity = 3 * tokens * top // (2 * n_ep)
    slots_per = -(-capacity // 16) * 16
    slots = n_ep * slots_per
    hidden_w = gate_weight.shape[2]
    out_w = mix_out_weight.shape[1]
    half = rows // n_tp
    vm = pltpu.VMEM
    dma = pltpu.SemaphoreType.DMA
    scratch = [
        vm(queries.shape, BF), vm((rows, LANES), BF), vm((rows, LANES), BF), vm((tokens, col_w), BF),
        vm((n_ep, rows, LANES), BF), vm((heads, rows, LANES), BF),
        vm((n_ep, slots_per, col_w), BF), vm((n_tp, n_ep, slots_per, col_w), BF),
        vm((slots, width), BF), vm((slots, hidden_w), BF),
        vm((width, hidden_w), BF), vm((width, hidden_w), BF), vm((hidden_w, width), BF),
        vm(mix_out_weight.shape, BF),
        vm((n_tp, slots, col_w), BF), vm((n_y, slots, col_w), BF), vm((n_y, slots, col_w), BF),
        vm((n_y, slots, col_w), BF),
        vm((n_ep, slots_per, col_w), BF), vm((n_ep, slots_per, col_w), BF),
        vm((n_y, 2, half, out_w), BF), vm((n_y, half, out_w), BF), vm((n_y, half, out_w), BF),
        vm((n_y, half, out_w), BF),
        dma((8,)),
        dma((n_ep,)), dma((n_ep,)), dma((n_ep,)), dma((n_ep,)),
        dma((n_y, n_ep)), dma((n_y, n_ep)),
    ] + [dma((n_y,))] * 6 + [dma((n_ep,))] * 2 + [dma((n_y,))] * 4
    in_vmem = pl.BlockSpec(memory_space=pltpu.VMEM)
    in_any = pl.BlockSpec(memory_space=pl.ANY)
    return pl.pallas_call(
        functools.partial(kernel, n_ep, n_tp, heads, width),
        out_shape=(
            jax.ShapeDtypeStruct((half, out_w), BF),
            jax.ShapeDtypeStruct((tokens, col_w), BF),
        ),
        in_specs=[in_any] * 3 + [in_vmem] * 2 + [in_any] * 2 + [in_vmem] * 3 + [in_any] * 3,
        out_specs=(in_vmem, in_vmem),
        scratch_shapes=scratch,
        compiler_params=pltpu.CompilerParams(
            collective_id=0, has_side_effects=True, vmem_limit_bytes=60 * 1024 * 1024
        ),
    )(
        queries, key_input, value_input, query_gain[None, :], key_gain[None, :],
        mix_out_weight, expert_input, ffn_gain[None, :], routes.T, route_scores.T,
        gate_weight, up_weight, down_weight,
    )


def solution(mesh):
    placed = (
        P("ep", "tp"),
        P("ep", None),
        P("ep", None),
        P(),
        P(),
        P("tp", None),
        P("ep", None),
        P(),
        P("ep", None),
        P("ep", None),
        P("ep", None, "tp"),
        P("ep", None, "tp"),
        P("ep", "tp", None),
    )
    return jax.shard_map(
        functools.partial(local, mesh.shape["ep"], mesh.shape["tp"]),
        mesh=mesh,
        in_specs=placed,
        out_specs=(P(("ep", "tp"), None), P("ep", "tp")),
        check_vma=False,
    )
```

profile of v0, /device:TPU:0, one launch (start us, length us, event | category | flops | bytes accessed | tf_op | source)
XLA Modules:
  0.0 69.3 jit_solution(13072696709541873627)
XLA Ops:
  0.6 65.2 %shard_map.140 = (bf16[128,2048]{1,0:T(8,128)(2,1)}, bf16[160,512]{1,0:T(8,128)(2,1)}) custom-call(bf16[512,256]{1,0:T(8,128)(2,1)} %q_any.1, bf16[512,256]{1,0:T(8,128)(2,1)} %k_any.1, bf16[512,256]{1,0:T(8,128)(2,1)} %v_any.1, f32[1,64]{1,0:T(1,128)} %bitcast.8, f32[1,64]{1,0:T(1,128)} %bitcast.9, bf16[256,2048]{1,0:T(8,128)(2,1)} %wmix_ref.1, ...), custom_call_target="tpu_custom_call" | custom-call | tf_op jit(solution)/shard_map/pallas_call | solution.py:492
  65.8 1.9 %copy.17 = bf16[128,2048]{1,0:T(8,128)(2,1)} copy(bf16[128,2048]{1,0:T(8,128)(2,1)} %get-tuple-element.4) | data formatting | bytes 1048576
  67.7 1.6 %copy.18 = bf16[160,512]{1,0:T(8,128)(2,1)} copy(bf16[160,512]{1,0:T(8,128)(2,1)} %get-tuple-element.5) | data formatting | bytes 327680
where the time goes:
time: 70.6 us; the launch traced here: 69.3 us
  Pallas kernels  65.2 us (92%)
  local copies, waits for them, and re-layouts  3.47 us (5%)
    pallas_call x1, Pallas kernels, local(): pl.pallas_call(functools.partial(kernel, n_ep, n_tp, heads, width), out_s...  65.2 us
    unnamed x2, local copies, waits for them, and re-layouts  3.47 us

commit v1 on v0

v1 whole, which is shorter than its diff:
```python
import functools
import math

import jax
import jax.numpy as jnp
from jax import lax
from jax.experimental import pallas as pl
from jax.experimental.pallas import tpu as pltpu
from jax.sharding import PartitionSpec as P

HEADS = 16
KV_HEADS = 4
HD = 64
GRID_W = 64
EPSILON = 1e-06
ROPE_BASE = 10000.0
MESH = pl.DeviceIdType.MESH
LANES = 128
BF = jnp.bfloat16
F32 = jnp.float32


def prep(values, gain, cos_table, sin_table):
    width = values.shape[1]
    squares = values * values
    high = squares.astype(BF)
    low = (squares - high.astype(F32)).astype(BF)
    rows = lax.broadcasted_iota(jnp.int32, (width, width), 0) // HD
    cols = lax.broadcasted_iota(jnp.int32, (width, width), 1) // HD
    same = jnp.where(rows == cols, 1.0, 0.0).astype(BF)
    total = jnp.dot(high, same, preferred_element_type=F32) + jnp.dot(
        low, same, preferred_element_type=F32
    )
    gain = jnp.concatenate([gain] * (width // HD), axis=1)
    normed = values * lax.rsqrt(total * (1.0 / HD) + EPSILON) * gain
    lane = lax.broadcasted_iota(jnp.int32, normed.shape, 1)
    quarter = HD // 4
    partner = jnp.where(
        lane % (2 * quarter) < quarter,
        pltpu.roll(normed, width - quarter, 1),
        pltpu.roll(normed, quarter, 1),
    )
    return normed * cos_table + partner * sin_table


def angle_tables(start, rows):
    quarter = HD // 4
    many = rows // GRID_W

    def both(count, first):
        shape = (count, LANES)
        place = lax.broadcasted_iota(jnp.int32, shape, 0) + first
        lane = lax.broadcasted_iota(jnp.int32, shape, 1)
        turn = lane % quarter
        inverse = jnp.zeros(shape, F32)
        for j in range(quarter):
            inverse = jnp.where(turn == j, ROPE_BASE ** (-j / quarter), inverse)
        angle = place.astype(F32) * inverse
        sign = jnp.where(lane % (2 * quarter) < quarter, -1.0, 1.0)
        return jnp.cos(angle), jnp.sin(angle) * sign

    tables = []
    for by_row, by_col in zip(both(max(many, 8), start // GRID_W), both(GRID_W, 0)):
        lane = lax.broadcasted_iota(jnp.int32, by_col.shape, 1)
        tables.append(
            jnp.concatenate(
                [jnp.where(lane % HD < HD // 2, by_row[i:i + 1, :], by_col) for i in range(many)],
                axis=0,
            )
        )
    return tables


def mark(name):
    pass


def kernel(
    n_ep, n_tp, heads, model_width,
    q_any, k_any, v_any, qg_any, kg_any, wmix_any, x_any, gain_any, routes_any, scores_any, wg_any, wu_any, wd_any,
    mixed_ref, out_ref,
    q_ref, k_in, v_in, x_ref, qg_ref, kg_ref, gain_ref, routes_ref, scores_ref, wg, wu, wd, wmix,
    kv_buf, q_buf, acc, x_out, x_buf, scaled, hid, dp_buf, ep_in, es_buf, ey_in,
    ret_out, ret_in, mp_out, mp_in, ms_out, my_in,
    w_sem, kvx_s, kvz_s, kv_r, di_s, di_r, dy_s, dy_r, dc_s, dc_r, ep_s, ep_r, ey_s, ey_r, rt_s, rt_r,
    mp_s, mp_r, my_s, my_r,
):
    n_y = n_tp // 2
    n_x = 1 << ((n_ep.bit_length() - 1) // 2)
    n_z = n_ep // n_x
    stages = n_z - 1
    me = lax.axis_index("ep")
    tp = lax.axis_index("tp")
    my_y, core = tp // 2, tp % 2
    my_z, my_x = me // n_x, me % n_x
    mate = my_y * 2 + 1 - core
    rows = q_ref.shape[0]
    kv_head = tp * heads // (HEADS // KV_HEADS)
    kv_tile = pl.ds(pl.multiple_of(kv_head // 2 * LANES, LANES), LANES)
    slots_per, col_w = x_buf.shape[2:]
    slots = n_ep * slots_per
    group = n_x * slots_per
    tokens = x_ref.shape[0]
    x_cols = pl.ds(pl.multiple_of(tp * col_w, col_w), col_w)

    def y_peer(j):
        return (my_y + j) % n_y

    def z_other(o):
        z = my_z
        for bit in range(n_z.bit_length() - 1):
            if o >> bit & 1:
                z = z + (1 - 2 * (my_z // (1 << bit) % 2)) * (1 << bit)
        return z

    def ep_other(o, i):
        return z_other(o) * n_x + (my_x + i) % n_x

    mark("a_greet")
    barrier = pltpu.get_barrier_semaphore()

    def greet(o, carry):
        pl.semaphore_signal(barrier, inc=1, device_id=((me + o) % n_ep, tp), device_id_type=MESH)
        return carry

    lax.fori_loop(1, n_ep, greet, 0)
    for j in range(1, n_y):
        pl.semaphore_signal(
            barrier, inc=1, device_id=(me, y_peer(j) * 2 + core), device_id_type=MESH
        )
    pl.semaphore_signal(barrier, inc=1, device_id=(me, mate), device_id_type=MESH)

    loads = [
        pltpu.make_async_copy(src, dst, w_sem.at[i])
        for i, (src, dst) in enumerate(
            (
                (routes_any, routes_ref),
                (x_any.at[:, x_cols], x_ref),
                (kg_any, kg_ref),
                (k_any.at[:, kv_tile], k_in),
                (v_any.at[:, kv_tile], v_in),
                (qg_any, qg_ref),
                (q_any, q_ref),
                (gain_any, gain_ref),
                (scores_any, scores_ref),
                (wg_any.at[0], wg),
                (wu_any.at[0], wu),
                (wd_any.at[0], wd),
                (wmix_any, wmix),
            )
        )
    ]
    for load in loads:
        load.start()

    mark("b_route")
    loads[0].wait()
    expert_row = lax.broadcasted_iota(jnp.int32, (n_ep, tokens), 0)
    first = jnp.where(expert_row == routes_ref[0:1, :], 1.0, 0.0)
    second = jnp.where(expert_row == routes_ref[1:2, :], 1.0, 0.0)
    earlier = jnp.where(
        lax.broadcasted_iota(jnp.int32, (tokens, tokens), 0)
        < lax.broadcasted_iota(jnp.int32, (tokens, tokens), 1),
        1.0,
        0.0,
    ).astype(BF)
    before = jnp.dot((first + second).astype(BF), earlier, preferred_element_type=F32)
    place = before + expert_row.astype(F32) * slots_per
    slot_a = jnp.sum(first * place, axis=0, keepdims=True).astype(jnp.int32)
    slot_b = jnp.sum(second * place, axis=0, keepdims=True).astype(jnp.int32)
    slot_row = lax.broadcasted_iota(jnp.int32, (slots, tokens), 0)
    pick_a = jnp.where(slot_row == slot_a, 1.0, 0.0).astype(BF)
    pick_b = jnp.where(slot_row == slot_b, 1.0, 0.0).astype(BF)
    mark("c_pack")
    loads[1].wait()
    sent = jnp.dot(pick_a + pick_b, x_ref[...], preferred_element_type=F32).astype(BF)
    x_out[...] = sent.reshape(x_out.shape)
    x_buf[tp, me] = x_out[me]

    mark("d_barrier")
    pl.semaphore_wait(barrier, n_ep - 1 + n_y)

    def disp(peer, source):
        return pltpu.make_async_remote_copy(
            x_out.at[peer], x_buf.at[tp, source], di_s.at[peer], di_r.at[source],
            device_id=(peer, tp), device_id_type=MESH,
        )

    def over_y(j, source, owner):
        return pltpu.make_async_remote_copy(
            x_buf.at[owner * 2 + core, source], x_buf.at[owner * 2 + core, source],
            dy_s.at[y_peer(j), source], dy_r.at[owner, source],
            device_id=(me, y_peer(j) * 2 + core), device_id_type=MESH,
        )

    mark("e_disp")
    for o in range(n_z):

        def start_disp(i, carry):
            disp(ep_other(o, i), me).start()
            return carry

        lax.fori_loop(1 if o == 0 else 0, n_x, start_disp, 0)
    for j in range(1, n_y):
        over_y(j, me, my_y).start()

    def x_peer(i):
        return my_z * n_x + (my_x + i) % n_x

    def kv_send(peer, origin, sem):
        return pltpu.make_async_remote_copy(
            kv_buf.at[origin], kv_buf.at[origin], sem, kv_r.at[origin],
            device_id=(peer, tp), device_id_type=MESH,
        )

    mark("f_prepk")
    cos_table, sin_table = angle_tables(me * rows, rows)
    for i in (2, 3, 4):
        loads[i].wait()
    odd = kv_head % 2 == 1
    key = k_in[...].astype(F32)
    value = v_in[...].astype(F32)
    key = jnp.where(odd, pltpu.roll(key, HD, 1), key)
    value = jnp.where(odd, value, pltpu.roll(value, HD, 1))
    turned = prep(key, kg_ref[...], cos_table, sin_table)
    lane = lax.broadcasted_iota(jnp.int32, key.shape, 1)
    kv_buf[me] = jnp.where(lane < HD, turned, value).astype(BF)

    def own_kv_right():
        return kv_send((my_z + 1) % n_z * n_x + my_x, me, kvz_s.at[my_z, 0])

    def own_kv_left():
        return kv_send((my_z + n_z - 1) % n_z * n_x + my_x, me, kvz_s.at[my_z, 1])

    for i in range(1, n_x):
        kv_send(x_peer(i), me, kvx_s.at[my_z, i]).start()

    @pl.when(my_z < n_z - 1)
    def _():
        own_kv_right().start()

    @pl.when(my_z > 0)
    def _():
        own_kv_left().start()

    side = my_z // (n_z // 2)
    outward = 1 - 2 * side
    inner = my_z + side * (n_z - 1 - 2 * my_z)

    def z_near(k):
        step = jnp.where(
            k <= 2 * inner, (k + 1) // 2 * (-1 if k % 2 else 1), k - inner
        )
        return my_z + outward * step

    def kv_onward(k):
        z = z_near(k)
        onward = my_z + jnp.where(z < my_z, 1, -1)
        inside = jnp.logical_and(onward >= 0, onward < n_z)
        peer = (onward + n_z) % n_z * n_x + my_x
        return inside, kv_send(peer, z * n_x + my_x, kvz_s.at[z, 0])

    def kv_forward(k):
        z = z_near(k)
        origin = z * n_x + my_x
        kv_send(origin, origin, kvz_s.at[z, 0]).wait_recv()
        inside, onward = kv_onward(k)

        @pl.when(inside)
        def _():
            onward.start()

        for i in range(1, n_x):
            kv_send(x_peer(i), origin, kvx_s.at[z, i]).start()

    mark("f_prepq")
    factor = HD ** (-0.5) * math.log2(math.e)
    loads[5].wait()
    loads[6].wait()
    for tile in range(q_ref.shape[1] // LANES):
        q_tile = factor * prep(
            q_ref[:, tile * LANES:(tile + 1) * LANES].astype(F32),
            qg_ref[...], cos_table, sin_table,
        )
        q_lane = lax.broadcasted_iota(jnp.int32, q_tile.shape, 1)
        for part in range(2):
            head = tile * 2 + part
            if head < heads:
                moved = q_tile if part == 0 else pltpu.roll(q_tile, HD, 1)
                q_buf[head] = jnp.where(q_lane < HD, moved, 0.0).astype(BF)

    piece = rows // n_y
    half = piece // 2

    def attend(block, owner, fresh=False):
        start = pl.multiple_of(owner * piece, piece)
        q_rows = q_buf[:, pl.ds(start, piece), :].reshape(heads * piece, LANES)
        kv = kv_buf[block]
        logits = lax.dot_general(
            q_rows, kv, (((1,), (1,)), ((), ())), preferred_element_type=F32
        )
        weights = jnp.exp2(logits).astype(BF)
        kv_lane = lax.broadcasted_iota(jnp.int32, kv.shape, 1)
        values = jnp.where(kv_lane < HD, jnp.ones_like(kv), kv)
        part = jnp.dot(weights, values, preferred_element_type=F32)
        acc[owner] = part if fresh else acc[owner] + part

    def attend_all(block, fresh=False):
        def one(owner, carry):
            attend(block, owner, fresh)
            return carry

        lax.fori_loop(0, n_y, one, 0)

    def kv_arrived(origin):
        kv_send(origin, origin, kvx_s.at[0, 0]).wait_recv()

    def others_attend(z):
        def one(i, carry):
            origin = z * n_x + (my_x + i) % n_x
            kv_arrived(origin)
            attend_all(origin)
            return carry

        lax.fori_loop(1, n_x, one, 0)

    def base(s):
        return my_z // 2 * 2 if s == 0 else z_other(s + 1)

    def many(s):
        return 2 if s == 0 else 1

    def members(s):
        return pl.ds(base(s) * n_x, many(s) * n_x)

    def stage_rows(s):
        return pl.ds(pl.multiple_of(base(s) * group, group), many(s) * group)

    def to_mate(owner, mine, s):
        part = x_buf.at[owner * 2 + mine, members(s)]
        return pltpu.make_async_remote_copy(
            part, part, dc_s.at[owner, s], dc_r.at[owner, s],
            device_id=(me, mate), device_id_type=MESH,
        )

    def pass_on(s):
        for o in (0, 1) if s == 0 else (s + 1,):

            def one(i, carry):
                source = ep_other(o, i)
                disp(source, source).wait_recv()
                for j in range(1, n_y):
                    over_y(j, source, my_y).start()
                return carry

            lax.fori_loop(1 if o == 0 else 0, n_x, one, 0)
        to_mate(my_y, core, s).start()

    def from_y(s):
        for j in range(1, n_y):
            owner = y_peer(j)

            def arrived(i, carry):
                over_y(j, base(s) * n_x + i, owner).wait_recv()
                return carry

            lax.fori_loop(0, many(s) * n_x, arrived, 0)
            to_mate(owner, core, s).start()

    def expert_in(s):
        for j in range(n_y):
            to_mate(y_peer(j), 1 - core, s).wait_recv()
        count = many(s) * group
        power = jnp.zeros((count, 1), F32)
        for q in range(n_tp):
            x_q = x_buf[q, members(s)].reshape(count, col_w).astype(F32)
            power = power + jnp.sum(x_q * x_q, axis=1, keepdims=True)
            scaled[stage_rows(s), q * col_w:(q + 1) * col_w] = (
                x_q * gain_ref[:, q * col_w:(q + 1) * col_w]
            ).astype(BF)
        return lax.rsqrt(power * (1.0 / model_width) + EPSILON)

    hidden_w = wg.shape[1]
    tile_w = math.gcd(hidden_w, 512)

    def expert_hidden(s, row_scale):
        at = stage_rows(s)

        def hidden_tile(i, carry):
            cols = pl.ds(pl.multiple_of(i * tile_w, tile_w), tile_w)
            gate = row_scale * jnp.dot(scaled[at, :], wg[:, cols], preferred_element_type=F32)
            up = row_scale * jnp.dot(scaled[at, :], wu[:, cols], preferred_element_type=F32)
            hid[at, cols] = (gate / (1.0 + jnp.exp(-gate)) * up).astype(BF)
            return carry

        lax.fori_loop(0, hidden_w // tile_w, hidden_tile, 0)

    def expert_mate(owner, side, s):
        return pltpu.make_async_remote_copy(
            dp_buf.at[owner * 2 + side, stage_rows(s)], ep_in.at[owner, stage_rows(s)],
            ep_s.at[owner, s], ep_r.at[owner, s],
            device_id=(me, mate), device_id_type=MESH,
        )

    def expert_y(j, origin, s):
        return pltpu.make_async_remote_copy(
            es_buf.at[y_peer(j), stage_rows(s)], ey_in.at[origin, stage_rows(s)],
            ey_s.at[y_peer(j), s], ey_r.at[origin, s],
            device_id=(me, y_peer(j) * 2 + core), device_id_type=MESH,
        )

    def expert_down(s):
        at = stage_rows(s)
        for whose in (1 - core, core):
            for j in range(1, n_y + 1):
                owner = y_peer(j)
                q = owner * 2 + whose
                cols = pl.ds(pl.multiple_of(q * col_w, col_w), col_w)
                dp_buf[q, at] = jnp.dot(
                    hid[at, :], wd[:, cols], preferred_element_type=F32
                ).astype(BF)
                if whose is not core:
                    expert_mate(owner, 1 - core, s).start()

    def mate_sum(j, s):
        owner = y_peer(j)
        expert_mate(owner, core, s).wait_recv()
        at = stage_rows(s)
        return dp_buf[owner * 2 + core, at].astype(F32) + ep_in[owner, at].astype(F32)

    def expert_send(s):
        for j in range(1, n_y):
            es_buf[y_peer(j), stage_rows(s)] = mate_sum(j, s).astype(BF)
            expert_y(j, my_y, s).start()

    def ret(peer, origin):
        return pltpu.make_async_remote_copy(
            ret_out.at[peer], ret_in.at[origin], rt_s.at[peer], rt_r.at[origin],
            device_id=(peer, tp), device_id_type=MESH,
        )

    def expert_return(s):
        total = mate_sum(0, s)
        for j in range(1, n_y):
            expert_y(j, y_peer(j), s).wait_recv()
            total = total + ey_in[y_peer(j), stage_rows(s)].astype(F32)
        ret_out[members(s)] = total.astype(BF).reshape(many(s) * n_x, slots_per, col_w)
        for o in (0, 1) if s == 0 else (s + 1,):

            def one(i, carry):
                ret(ep_other(o, i), me).start()
                return carry

            lax.fori_loop(1 if o == 0 else 0, n_x, one, 0)
        if s == 0:
            ret_in[me] = ret_out[me]

    def mix_mate(owner, side):
        return pltpu.make_async_remote_copy(
            mp_out.at[owner, side], mp_in.at[owner], mp_s.at[owner], mp_r.at[owner],
            device_id=(me, mate), device_id_type=MESH,
        )

    def mix_y(j, origin):
        return pltpu.make_async_remote_copy(
            ms_out.at[y_peer(j)], my_in.at[origin], my_s.at[y_peer(j)], my_r.at[origin],
            device_id=(me, y_peer(j) * 2 + core), device_id_type=MESH,
        )

    def mix(owner):
        total = acc[owner]
        ratio = (total / pltpu.roll(total, HD, 1)).reshape(heads, piece, LANES)
        out_lane = lax.broadcasted_iota(jnp.int32, (piece, LANES), 1)
        tiles = []
        for tile in range(q_ref.shape[1] // LANES):
            left = pltpu.roll(ratio[2 * tile], HD, 1)
            right = ratio[2 * tile + 1] if 2 * tile + 1 < heads else jnp.zeros_like(left)
            tiles.append(jnp.where(out_lane < HD, left, right).astype(BF))
        attended = tiles[0] if len(tiles) == 1 else jnp.concatenate(tiles, axis=1)
        part = jnp.dot(attended, wmix[...], preferred_element_type=F32).astype(BF)
        mp_out[owner] = part.reshape(2, half, part.shape[1])
        mix_mate(owner, 1 - core).start()

    def mix_sum(owner):
        mix_mate(owner, core).wait_recv()
        return mp_out[owner, core].astype(F32) + mp_in[owner].astype(F32)

    mark("g_pass0")
    pass_on(0)
    mark("g_attown")
    attend_all(me, True)
    mark("g_attownx")
    others_attend(my_z)
    mark("g_kvf1")
    kv_forward(1)
    mark("g_fromy0")
    from_y(0)
    mark("g_att1")
    attend_all(z_near(1) * n_x + my_x)
    mark("h_in0")
    loads[7].wait()
    row_scale = expert_in(0)
    mark("h_hid0")
    loads[9].wait()
    loads[10].wait()
    expert_hidden(0, row_scale)
    mark("h_pass1")
    if stages > 1:
        pass_on(1)
    mark("h_down0")
    loads[11].wait()
    expert_down(0)
    mark("h_kvf2")
    if n_z > 2:
        kv_forward(2)
    mark("h_att1x")
    others_attend(z_near(1))
    mark("h_send0")
    expert_send(0)
    for s in range(1, stages):
        mark(f"i_fromy{s}")
        from_y(s)
        mark(f"i_kvf{s+2}")
        if s + 2 < n_z:
            kv_forward(s + 2)
        mark(f"i_in{s}")
        row_scale = expert_in(s)
        mark(f"i_hid{s}")
        expert_hidden(s, row_scale)
        mark(f"i_pass{s+1}")
        if s + 1 < stages:
            pass_on(s + 1)
        mark(f"i_down{s}")
        expert_down(s)
        mark(f"i_ret{s-1}")
        expert_return(s - 1)
        mark(f"i_send{s}")
        expert_send(s)

    mark("j_farkv")

    def far_attend(owner):
        for k in range(2, n_z):
            z = z_near(k)

            def one(i, carry):
                attend(z * n_x + (my_x + i) % n_x, owner)
                return carry

            lax.fori_loop(0, n_x, one, 0)

    for k in range(2, n_z):
        for i in range(1, n_x):
            kv_arrived(z_near(k) * n_x + (my_x + i) % n_x)
    mark("j_loadmix")
    loads[12].wait()
    for j in range(1, n_y):
        mark("j_att")
        far_attend(y_peer(j))
        if j == 1:
            mark("j_ret")
            expert_return(stages - 1)
        mark("j_mix")
        mix(y_peer(j))
    mark("k_att")
    far_attend(my_y)
    for j in range(1, n_y):
        mark("k_mixsum")
        ms_out[y_peer(j)] = mix_sum(y_peer(j)).astype(BF)
        mix_y(j, my_y).start()
    mark("k_mix")
    mix(my_y)

    mark("l_retwait")

    def ret_wait(o, carry):
        source = (me + n_ep - o) % n_ep
        ret(source, source).wait_recv()
        return carry

    lax.fori_loop(1, n_ep, ret_wait, 0)
    mark("m_combine")
    loads[8].wait()
    back = ret_in[...].reshape(slots, col_w)
    share_row = scores_ref[...] / jnp.sum(scores_ref[...], axis=0, keepdims=True)
    own_token = lax.broadcasted_iota(jnp.int32, (tokens, tokens), 0) == lax.broadcasted_iota(
        jnp.int32, (tokens, tokens), 1
    )
    share_a, share_b = (
        jnp.sum(jnp.where(own_token, share_row[i:i + 1, :], 0.0), axis=1, keepdims=True)
        for i in range(2)
    )
    rows_a = lax.dot_general(
        pick_a, back, (((0,), (0,)), ((), ())), preferred_element_type=F32
    )
    rows_b = lax.dot_general(
        pick_b, back, (((0,), (0,)), ((), ())), preferred_element_type=F32
    )
    out_ref[...] = (rows_a * share_a + rows_b * share_b).astype(BF)

    mark("n_mixsum")
    total = mix_sum(my_y)
    mark("n_ywait")
    for j in range(1, n_y):
        mix_y(j, y_peer(j)).wait_recv()
        total = total + my_in[y_peer(j)].astype(F32)
    mark("n_out")
    mixed_ref[...] = total.astype(BF)

    mark("o_sends")

    def sends(o, carry):
        peer = (me + o) % n_ep
        disp(peer, me).wait_send()
        ret(peer, me).wait_send()
        return carry

    lax.fori_loop(1, n_ep, sends, 0)
    for i in range(1, n_x):

        def sent_x(z, carry):
            kv_send(x_peer(i), z * n_x + my_x, kvx_s.at[z, i]).wait_send()
            return carry

        lax.fori_loop(0, n_z, sent_x, 0)

    @pl.when(my_z < n_z - 1)
    def _():
        own_kv_right().wait_send()

    @pl.when(my_z > 0)
    def _():
        own_kv_left().wait_send()

    for k in range(1, n_z):
        inside, onward = kv_onward(k)

        @pl.when(inside)
        def _():
            onward.wait_send()

    for j in range(1, n_y):

        def sent_y(source, carry):
            over_y(j, source, my_y).wait_send()
            return carry

        lax.fori_loop(0, n_ep, sent_y, 0)
        mix_y(j, my_y).wait_send()
    for j in range(n_y):
        for s in range(stages):
            to_mate(y_peer(j), core, s).wait_send()
            expert_mate(y_peer(j), 1 - core, s).wait_send()
            if j:
                expert_y(j, my_y, s).wait_send()
        mix_mate(y_peer(j), 1 - core).wait_send()
    mark(None)


def local(
    n_ep, n_tp,
    queries, key_input, value_input, query_gain, key_gain, mix_out_weight, expert_input, ffn_gain,
    routes, route_scores, gate_weight, up_weight, down_weight,
):
    rows = queries.shape[0]
    heads = queries.shape[1] // HD
    n_y = n_tp // 2
    n_x = 1 << ((n_ep.bit_length() - 1) // 2)
    n_z = n_ep // n_x
    stages = n_z - 1
    spare = heads % 2 * HD
    if spare:
        queries = jnp.pad(queries, ((0, 0), (0, spare)))
        mix_out_weight = jnp.pad(mix_out_weight, ((0, spare), (0, 0)))
    width = expert_input.shape[1]
    col_w = width // n_tp
    tokens, top = routes.shape
    capacity = 3 * tokens * top // (2 * n_ep)
    slots_per = -(-capacity // 16) * 16
    slots = n_ep * slots_per
    hidden_w = gate_weight.shape[2]
    out_w = mix_out_weight.shape[1]
    half = rows // n_tp
    vm = pltpu.VMEM
    dma = pltpu.SemaphoreType.DMA
    scratch = [
        vm(queries.shape, BF), vm((rows, LANES), BF), vm((rows, LANES), BF), vm((tokens, col_w), BF),
        vm((1, HD), F32), vm((1, HD), F32), vm((1, width), F32), vm((top, tokens), jnp.int32), vm((top, tokens), F32),
        vm((width, hidden_w), BF), vm((width, hidden_w), BF), vm((hidden_w, width), BF),
        vm(mix_out_weight.shape, BF),
        vm((n_ep, rows, LANES), BF), vm((heads, rows, LANES), BF), vm((n_y, heads * rows // n_y, LANES), F32),
        vm((n_ep, slots_per, col_w), BF), vm((n_tp, n_ep, slots_per, col_w), BF),
        vm((slots, width), BF), vm((slots, hidden_w), BF),
        vm((n_tp, slots, col_w), BF), vm((n_y, slots, col_w), BF), vm((n_y, slots, col_w), BF),
        vm((n_y, slots, col_w), BF),
        vm((n_ep, slots_per, col_w), BF), vm((n_ep, slots_per, col_w), BF),
        vm((n_y, 2, half, out_w), BF), vm((n_y, half, out_w), BF), vm((n_y, half, out_w), BF),
        vm((n_y, half, out_w), BF),
        dma((13,)),
        dma((n_z, n_x)), dma((n_z, 2)), dma((n_ep,)), dma((n_ep,)), dma((n_ep,)),
        dma((n_y, n_ep)), dma((n_y, n_ep)),
    ] + [dma((n_y, stages))] * 6 + [dma((n_ep,))] * 2 + [dma((n_y,))] * 4
    in_vmem = pl.BlockSpec(memory_space=pltpu.VMEM)
    in_hbm = pl.BlockSpec(memory_space=pltpu.HBM)
    return pl.pallas_call(
        functools.partial(kernel, n_ep, n_tp, heads, width),
        out_shape=(
            jax.ShapeDtypeStruct((half, out_w), BF),
            jax.ShapeDtypeStruct((tokens, col_w), BF),
        ),
        in_specs=[in_hbm] * 13,
        out_specs=(in_vmem, in_vmem),
        scratch_shapes=scratch,
        compiler_params=pltpu.CompilerParams(
            collective_id=0, has_side_effects=True, vmem_limit_bytes=60 * 1024 * 1024
        ),
    )(
        queries, key_input, value_input, query_gain[None, :], key_gain[None, :],
        mix_out_weight, expert_input, ffn_gain[None, :], routes.T, route_scores.T,
        gate_weight, up_weight, down_weight,
    )


def solution(mesh):
    placed = (
        P("ep", "tp"),
        P("ep", None),
        P("ep", None),
        P(),
        P(),
        P("tp", None),
        P("ep", None),
        P(),
        P("ep", None),
        P("ep", None),
        P("ep", None, "tp"),
        P("ep", None, "tp"),
        P("ep", "tp", None),
    )
    return jax.shard_map(
        functools.partial(local, mesh.shape["ep"], mesh.shape["tp"]),
        mesh=mesh,
        in_specs=placed,
        out_specs=(P(("ep", "tp"), None), P("ep", "tp")),
        check_vma=False,
    )
```

time: 70.6 us -> 75 us (1.062); the launches traced: 69.3 us -> 74.9 us
  Pallas kernels: 65.2 us -> 70.7 us
    pallas_call x1, Pallas kernels: 65.2 us -> 70.7 us  [local(): pl.pallas_call(functools.partial(kernel, n_ep, n_tp, heads, width), out_s...]
where the time goes in v1:
time: 75 us; the launch traced here: 74.9 us
  Pallas kernels  70.7 us (94%)
  local copies, waits for them, and re-layouts  3.47 us (5%)
    pallas_call x1, Pallas kernels, local(): pl.pallas_call(functools.partial(kernel, n_ep, n_tp, heads, width), out_s...  70.7 us
    unnamed x2, local copies, waits for them, and re-layouts  3.47 us

profile of v1, /device:TPU:0, one launch (start us, length us, event | category | flops | bytes accessed | tf_op | source)
XLA Modules:
  0.0 74.9 jit_solution(10182250643875956449)
XLA Ops:
  0.6 70.7 %shard_map.140 = (bf16[128,2048]{1,0:T(8,128)(2,1)}, bf16[160,512]{1,0:T(8,128)(2,1)}) custom-call(bf16[512,256]{1,0:T(8,128)(2,1)} %q_any.1, bf16[512,256]{1,0:T(8,128)(2,1)} %k_any.1, bf16[512,256]{1,0:T(8,128)(2,1)} %v_any.1, f32[1,64]{1,0:T(1,128)} %bitcast.8, f32[1,64]{1,0:T(1,128)} %bitcast.9, bf16[256,2048]{1,0:T(8,128)(2,1)} %wmix_any.1, ...), custom_call_target="tpu_custom_call" | custom-call | tf_op jit(solution)/shard_map/pallas_call | solution.py:705
  71.4 1.9 %copy.17 = bf16[128,2048]{1,0:T(8,128)(2,1)} copy(bf16[128,2048]{1,0:T(8,128)(2,1)} %get-tuple-element.4) | data formatting | bytes 1048576
  73.3 1.6 %copy.18 = bf16[160,512]{1,0:T(8,128)(2,1)} copy(bf16[160,512]{1,0:T(8,128)(2,1)} %get-tuple-element.5) | data formatting | bytes 327680

commit v2 on v1

--- a/solution.py
+++ b/solution.py
@@ -88,7 +88,7 @@
     n_y = n_tp // 2
     n_x = 1 << ((n_ep.bit_length() - 1) // 2)
     n_z = n_ep // n_x
-    stages = n_z - 1
+    stages = n_z
     me = lax.axis_index("ep")
     tp = lax.axis_index("tp")
     my_y, core = tp // 2, tp % 2
@@ -115,20 +115,6 @@
 
     def ep_other(o, i):
         return z_other(o) * n_x + (my_x + i) % n_x
-
-    mark("a_greet")
-    barrier = pltpu.get_barrier_semaphore()
-
-    def greet(o, carry):
-        pl.semaphore_signal(barrier, inc=1, device_id=((me + o) % n_ep, tp), device_id_type=MESH)
-        return carry
-
-    lax.fori_loop(1, n_ep, greet, 0)
-    for j in range(1, n_y):
-        pl.semaphore_signal(
-            barrier, inc=1, device_id=(me, y_peer(j) * 2 + core), device_id_type=MESH
-        )
-    pl.semaphore_signal(barrier, inc=1, device_id=(me, mate), device_id_type=MESH)
 
     loads = [
         pltpu.make_async_copy(src, dst, w_sem.at[i])
@@ -152,6 +138,20 @@
     ]
     for load in loads:
         load.start()
+
+    mark("a_greet")
+    barrier = pltpu.get_barrier_semaphore()
+
+    def greet(o, carry):
+        pl.semaphore_signal(barrier, inc=1, device_id=((me + o) % n_ep, tp), device_id_type=MESH)
+        return carry
+
+    lax.fori_loop(1, n_ep, greet, 0)
+    for j in range(1, n_y):
+        pl.semaphore_signal(
+            barrier, inc=1, device_id=(me, y_peer(j) * 2 + core), device_id_type=MESH
+        )
+    pl.semaphore_signal(barrier, inc=1, device_id=(me, mate), device_id_type=MESH)
 
     mark("b_route")
     loads[0].wait()
@@ -177,9 +177,6 @@
     x_out[...] = sent.reshape(x_out.shape)
     x_buf[tp, me] = x_out[me]
 
-    mark("d_barrier")
-    pl.semaphore_wait(barrier, n_ep - 1 + n_y)
-
     def disp(peer, source):
         return pltpu.make_async_remote_copy(
             x_out.at[peer], x_buf.at[tp, source], di_s.at[peer], di_r.at[source],
@@ -193,17 +190,6 @@
             device_id=(me, y_peer(j) * 2 + core), device_id_type=MESH,
         )
 
-    mark("e_disp")
-    for o in range(n_z):
-
-        def start_disp(i, carry):
-            disp(ep_other(o, i), me).start()
-            return carry
-
-        lax.fori_loop(1 if o == 0 else 0, n_x, start_disp, 0)
-    for j in range(1, n_y):
-        over_y(j, me, my_y).start()
-
     def x_peer(i):
         return my_z * n_x + (my_x + i) % n_x
 
@@ -212,6 +198,35 @@
             kv_buf.at[origin], kv_buf.at[origin], sem, kv_r.at[origin],
             device_id=(peer, tp), device_id_type=MESH,
         )
+
+    def own_kv_right():
+        return kv_send((my_z + 1) % n_z * n_x + my_x, me, kvz_s.at[my_z, 0])
+
+    def own_kv_left():
+        return kv_send((my_z + n_z - 1) % n_z * n_x + my_x, me, kvz_s.at[my_z, 1])
+
+    mark("d_barrier")
+    pl.semaphore_wait(barrier, n_ep - 1 + n_y)
+
+    mark("e_disp")
+    def dispatch(o):
+        def start_disp(i, carry):
+            disp(ep_other(o, i), me).start()
+            return carry
+
+        lax.fori_loop(1 if o == 0 else 0, n_x, start_disp, 0)
+
+    at_end = jnp.logical_or(my_z == 0, my_z == n_z - 1)
+    dispatch(0)
+    dispatch(1)
+
+    @pl.when(jnp.logical_not(at_end))
+    def _():
+        for o in range(2, n_z):
+            dispatch(o)
+
+    for j in range(1, n_y):
+        over_y(j, me, my_y).start()
 
     mark("f_prepk")
     cos_table, sin_table = angle_tables(me * rows, rows)
@@ -226,12 +241,6 @@
     lane = lax.broadcasted_iota(jnp.int32, key.shape, 1)
     kv_buf[me] = jnp.where(lane < HD, turned, value).astype(BF)
 
-    def own_kv_right():
-        return kv_send((my_z + 1) % n_z * n_x + my_x, me, kvz_s.at[my_z, 0])
-
-    def own_kv_left():
-        return kv_send((my_z + n_z - 1) % n_z * n_x + my_x, me, kvz_s.at[my_z, 1])
-
     for i in range(1, n_x):
         kv_send(x_peer(i), me, kvx_s.at[my_z, i]).start()
 
@@ -243,6 +252,11 @@
     def _():
         own_kv_left().start()
 
+    @pl.when(at_end)
+    def _():
+        for o in range(2, n_z):
+            dispatch(o)
+
     side = my_z // (n_z // 2)
     outward = 1 - 2 * side
     inner = my_z + side * (n_z - 1 - 2 * my_z)
@@ -253,25 +267,25 @@
         )
         return my_z + outward * step
 
-    def kv_onward(k):
-        z = z_near(k)
-        onward = my_z + jnp.where(z < my_z, 1, -1)
-        inside = jnp.logical_and(onward >= 0, onward < n_z)
-        peer = (onward + n_z) % n_z * n_x + my_x
-        return inside, kv_send(peer, z * n_x + my_x, kvz_s.at[z, 0])
-
-    def kv_forward(k):
-        z = z_near(k)
+    def kv_pass(t, way):
+        z = my_z - way * t
+        there = jnp.logical_and(z >= 0, z < n_z)
+        onward = my_z + way
+        beyond = jnp.logical_and(onward >= 0, onward < n_z)
+        z, onward = (z + n_z) % n_z, (onward + n_z) % n_z
+        return there, beyond, z, kv_send(onward * n_x + my_x, z * n_x + my_x, kvz_s.at[z, 0])
+
+    def kv_forward(t, way, ends):
+        there, beyond, z, onward = kv_pass(t, way)
         origin = z * n_x + my_x
-        kv_send(origin, origin, kvz_s.at[z, 0]).wait_recv()
-        inside, onward = kv_onward(k)
-
-        @pl.when(inside)
+
+        @pl.when(jnp.logical_and(there, jnp.logical_not(beyond) if ends else beyond))
         def _():
-            onward.start()
-
-        for i in range(1, n_x):
-            kv_send(x_peer(i), origin, kvx_s.at[z, i]).start()
+            kv_send(origin, origin, kvz_s.at[z, 0]).wait_recv()
+            if not ends:
+                onward.start()
+            for i in range(1, n_x):
+                kv_send(x_peer(i), origin, kvx_s.at[z, i]).start()
 
     mark("f_prepq")
     factor = HD ** (-0.5) * math.log2(math.e)
@@ -291,23 +305,24 @@
 
     piece = rows // n_y
     half = piece // 2
-
-    def attend(block, owner, fresh=False):
-        start = pl.multiple_of(owner * piece, piece)
-        q_rows = q_buf[:, pl.ds(start, piece), :].reshape(heads * piece, LANES)
-        kv = kv_buf[block]
+    pieces = my_s.shape[1]
+
+    def attend(block, count, start, many, fresh=False):
+        at = pl.ds(pl.multiple_of(start, half), many)
+        q_rows = q_buf[:, at, :].reshape(heads * many, LANES)
+        kv = kv_buf[pl.ds(block, count)].reshape(count * rows, LANES)
         logits = lax.dot_general(
             q_rows, kv, (((1,), (1,)), ((), ())), preferred_element_type=F32
         )
         weights = jnp.exp2(logits).astype(BF)
         kv_lane = lax.broadcasted_iota(jnp.int32, kv.shape, 1)
         values = jnp.where(kv_lane < HD, jnp.ones_like(kv), kv)
-        part = jnp.dot(weights, values, preferred_element_type=F32)
-        acc[owner] = part if fresh else acc[owner] + part
+        part = jnp.dot(weights, values, preferred_element_type=F32).reshape(heads, many, LANES)
+        acc[:, at, :] = part if fresh else acc[:, at, :] + part
 
     def attend_all(block, fresh=False):
         def one(owner, carry):
-            attend(block, owner, fresh)
+            attend(block, 1, owner * piece, piece, fresh)
             return carry
 
         lax.fori_loop(0, n_y, one, 0)
@@ -324,17 +339,11 @@
 
         lax.fori_loop(1, n_x, one, 0)
 
-    def base(s):
-        return my_z // 2 * 2 if s == 0 else z_other(s + 1)
-
-    def many(s):
-        return 2 if s == 0 else 1
-
     def members(s):
-        return pl.ds(base(s) * n_x, many(s) * n_x)
-
-    def stage_rows(s):
-        return pl.ds(pl.multiple_of(base(s) * group, group), many(s) * group)
+        return pl.ds(z_other(s) * n_x, n_x)
+
+    def group_rows(o):
+        return pl.ds(pl.multiple_of(z_other(o) * group, group), group)
 
     def to_mate(owner, mine, s):
         part = x_buf.at[owner * 2 + mine, members(s)]
@@ -343,48 +352,46 @@
             device_id=(me, mate), device_id_type=MESH,
         )
 
-    def pass_on(s):
-        for o in (0, 1) if s == 0 else (s + 1,):
-
-            def one(i, carry):
-                source = ep_other(o, i)
-                disp(source, source).wait_recv()
-                for j in range(1, n_y):
-                    over_y(j, source, my_y).start()
-                return carry
-
-            lax.fori_loop(1 if o == 0 else 0, n_x, one, 0)
-        to_mate(my_y, core, s).start()
+    def pass_on(o):
+        def one(i, carry):
+            source = ep_other(o, i)
+            disp(source, source).wait_recv()
+            for j in range(1, n_y):
+                over_y(j, source, my_y).start()
+            return carry
+
+        lax.fori_loop(1 if o == 0 else 0, n_x, one, 0)
+        to_mate(my_y, core, o).start()
 
     def from_y(s):
         for j in range(1, n_y):
             owner = y_peer(j)
 
             def arrived(i, carry):
-                over_y(j, base(s) * n_x + i, owner).wait_recv()
+                over_y(j, z_other(s) * n_x + i, owner).wait_recv()
                 return carry
 
-            lax.fori_loop(0, many(s) * n_x, arrived, 0)
+            lax.fori_loop(0, n_x, arrived, 0)
             to_mate(owner, core, s).start()
 
     def expert_in(s):
         for j in range(n_y):
             to_mate(y_peer(j), 1 - core, s).wait_recv()
-        count = many(s) * group
+        count = group
         power = jnp.zeros((count, 1), F32)
         for q in range(n_tp):
             x_q = x_buf[q, members(s)].reshape(count, col_w).astype(F32)
             power = power + jnp.sum(x_q * x_q, axis=1, keepdims=True)
-            scaled[stage_rows(s), q * col_w:(q + 1) * col_w] = (
+            scaled[group_rows(s), q * col_w:(q + 1) * col_w] = (
                 x_q * gain_ref[:, q * col_w:(q + 1) * col_w]
             ).astype(BF)
         return lax.rsqrt(power * (1.0 / model_width) + EPSILON)
 
     hidden_w = wg.shape[1]
-    tile_w = math.gcd(hidden_w, 512)
+    tile_w = math.gcd(hidden_w, 1024)
 
     def expert_hidden(s, row_scale):
-        at = stage_rows(s)
+        at = group_rows(s)
 
         def hidden_tile(i, carry):
             cols = pl.ds(pl.multiple_of(i * tile_w, tile_w), tile_w)
@@ -395,42 +402,37 @@
 
         lax.fori_loop(0, hidden_w // tile_w, hidden_tile, 0)
 
-    def expert_mate(owner, side, s):
+    def expert_mate(owner, side, o):
         return pltpu.make_async_remote_copy(
-            dp_buf.at[owner * 2 + side, stage_rows(s)], ep_in.at[owner, stage_rows(s)],
-            ep_s.at[owner, s], ep_r.at[owner, s],
+            dp_buf.at[owner * 2 + side, group_rows(o)], ep_in.at[owner, group_rows(o)],
+            ep_s.at[owner, o], ep_r.at[owner, o],
             device_id=(me, mate), device_id_type=MESH,
         )
 
-    def expert_y(j, origin, s):
+    def expert_y(j, origin, o):
         return pltpu.make_async_remote_copy(
-            es_buf.at[y_peer(j), stage_rows(s)], ey_in.at[origin, stage_rows(s)],
-            ey_s.at[y_peer(j), s], ey_r.at[origin, s],
+            es_buf.at[y_peer(j), group_rows(o)], ey_in.at[origin, group_rows(o)],
+            ey_s.at[y_peer(j), o], ey_r.at[origin, o],
             device_id=(me, y_peer(j) * 2 + core), device_id_type=MESH,
         )
 
     def expert_down(s):
-        at = stage_rows(s)
-        for whose in (1 - core, core):
-            for j in range(1, n_y + 1):
-                owner = y_peer(j)
-                q = owner * 2 + whose
-                cols = pl.ds(pl.multiple_of(q * col_w, col_w), col_w)
-                dp_buf[q, at] = jnp.dot(
-                    hid[at, :], wd[:, cols], preferred_element_type=F32
-                ).astype(BF)
-                if whose is not core:
-                    expert_mate(owner, 1 - core, s).start()
-
-    def mate_sum(j, s):
+        at = group_rows(s)
+        total = jnp.dot(hid[at, :], wd[...], preferred_element_type=F32).astype(BF)
+        for q in range(n_tp):
+            dp_buf[q, at] = total[:, q * col_w:(q + 1) * col_w]
+        for j in range(1, n_y + 1):
+            expert_mate(y_peer(j), 1 - core, s).start()
+
+    def mate_sum(j, o):
         owner = y_peer(j)
-        expert_mate(owner, core, s).wait_recv()
-        at = stage_rows(s)
+        expert_mate(owner, core, o).wait_recv()
+        at = group_rows(o)
         return dp_buf[owner * 2 + core, at].astype(F32) + ep_in[owner, at].astype(F32)
 
     def expert_send(s):
         for j in range(1, n_y):
-            es_buf[y_peer(j), stage_rows(s)] = mate_sum(j, s).astype(BF)
+            es_buf[y_peer(j), group_rows(s)] = mate_sum(j, s).astype(BF)
             expert_y(j, my_y, s).start()
 
     def ret(peer, origin):
@@ -439,20 +441,19 @@
             device_id=(peer, tp), device_id_type=MESH,
         )
 
-    def expert_return(s):
-        total = mate_sum(0, s)
+    def expert_return(o):
+        total = mate_sum(0, o)
         for j in range(1, n_y):
-            expert_y(j, y_peer(j), s).wait_recv()
-            total = total + ey_in[y_peer(j), stage_rows(s)].astype(F32)
-        ret_out[members(s)] = total.astype(BF).reshape(many(s) * n_x, slots_per, col_w)
-        for o in (0, 1) if s == 0 else (s + 1,):
-
-            def one(i, carry):
-                ret(ep_other(o, i), me).start()
-                return carry
-
-            lax.fori_loop(1 if o == 0 else 0, n_x, one, 0)
-        if s == 0:
+            expert_y(j, y_peer(j), o).wait_recv()
+            total = total + ey_in[y_peer(j), group_rows(o)].astype(F32)
+        ret_out[pl.ds(z_other(o) * n_x, n_x)] = total.astype(BF).reshape(n_x, slots_per, col_w)
+
+        def one(i, carry):
+            ret(ep_other(o, i), me).start()
+            return carry
+
+        lax.fori_loop(0 if o else 1, n_x, one, 0)
+        if o == 0:
             ret_in[me] = ret_out[me]
 
     def mix_mate(owner, side):
@@ -461,115 +462,168 @@
             device_id=(me, mate), device_id_type=MESH,
         )
 
-    def mix_y(j, origin):
+    def mix_y(j, origin, c):
+        at = pl.ds(c * (half // pieces), half // pieces)
         return pltpu.make_async_remote_copy(
-            ms_out.at[y_peer(j)], my_in.at[origin], my_s.at[y_peer(j)], my_r.at[origin],
+            ms_out.at[y_peer(j), at], my_in.at[origin, at], my_s.at[y_peer(j), c], my_r.at[origin, c],
             device_id=(me, y_peer(j) * 2 + core), device_id_type=MESH,
         )
 
-    def mix(owner):
-        total = acc[owner]
-        ratio = (total / pltpu.roll(total, HD, 1)).reshape(heads, piece, LANES)
-        out_lane = lax.broadcasted_iota(jnp.int32, (piece, LANES), 1)
+    def mix(owner, whose):
+        start = pl.multiple_of(owner * piece + whose * half, half)
+        total = acc[:, pl.ds(start, half), :].reshape(heads * half, LANES)
+        ratio = (total / pltpu.roll(total, HD, 1)).reshape(heads, half, LANES)
+        out_lane = lax.broadcasted_iota(jnp.int32, (half, LANES), 1)
         tiles = []
         for tile in range(q_ref.shape[1] // LANES):
             left = pltpu.roll(ratio[2 * tile], HD, 1)
             right = ratio[2 * tile + 1] if 2 * tile + 1 < heads else jnp.zeros_like(left)
             tiles.append(jnp.where(out_lane < HD, left, right).astype(BF))
         attended = tiles[0] if len(tiles) == 1 else jnp.concatenate(tiles, axis=1)
-        part = jnp.dot(attended, wmix[...], preferred_element_type=F32).astype(BF)
-        mp_out[owner] = part.reshape(2, half, part.shape[1])
-        mix_mate(owner, 1 - core).start()
+        mp_out[owner, whose] = jnp.dot(attended, wmix[...], preferred_element_type=F32).astype(BF)
 
     def mix_sum(owner):
         mix_mate(owner, core).wait_recv()
         return mp_out[owner, core].astype(F32) + mp_in[owner].astype(F32)
 
+    def near_arrived(k):
+        for i in range(1, n_x):
+            kv_arrived(z_near(k) * n_x + (my_x + i) % n_x)
+
+    others = [y_peer(j) for j in range(1, n_y)]
+
+    def attend_first(k, owners):
+        for owner in owners:
+            attend(z_near(k) * n_x + my_x, 1, owner * piece, piece)
+
+    def attend_second(k, owners):
+        def one(i, carry):
+            for owner in owners:
+                attend(z_near(k) * n_x + (my_x + i) % n_x, 1, owner * piece, piece)
+            return carry
+
+        lax.fori_loop(1, n_x, one, 0)
+
+    def attend_both(k, start, many):
+        attend(z_near(k) * n_x, n_x, start, many)
+
+    def expert_rows(s):
+        mark(f"in{s}")
+        row_scale = expert_in(s)
+        mark(f"hid{s}")
+        expert_hidden(s, row_scale)
+
+    mark("g_attown")
+    attend_all(me, True)
     mark("g_pass0")
     pass_on(0)
-    mark("g_attown")
-    attend_all(me, True)
-    mark("g_attownx")
+    mark("g_pass1")
+    pass_on(1)
+    mark("fromy0")
+    from_y(0)
+    mark("kva")
+    kv_forward(1, outward, False)
+    kv_forward(1, -outward, True)
+    mark("attownx")
     others_attend(my_z)
-    mark("g_kvf1")
-    kv_forward(1)
-    mark("g_fromy0")
-    from_y(0)
-    mark("g_att1")
-    attend_all(z_near(1) * n_x + my_x)
-    mark("h_in0")
     loads[7].wait()
-    row_scale = expert_in(0)
-    mark("h_hid0")
     loads[9].wait()
     loads[10].wait()
-    expert_hidden(0, row_scale)
-    mark("h_pass1")
-    if stages > 1:
-        pass_on(1)
-    mark("h_down0")
     loads[11].wait()
+    expert_rows(0)
+    mark("fromy1")
+    from_y(1)
+    mark("pass2")
+    pass_on(2)
+    mark("down0")
     expert_down(0)
-    mark("h_kvf2")
-    if n_z > 2:
-        kv_forward(2)
-    mark("h_att1x")
-    others_attend(z_near(1))
-    mark("h_send0")
+    mark("in1")
+    row_scale = expert_in(1)
+    mark("kvf1")
+    kv_forward(1, -outward, False)
+    mark("hid1")
+    expert_hidden(1, row_scale)
+    mark("pass3")
+    pass_on(3)
+    mark("down1")
+    expert_down(1)
+    mark("att1")
+    attend_first(1, others)
+    mark("send0")
     expert_send(0)
-    for s in range(1, stages):
-        mark(f"i_fromy{s}")
+    for s in range(2, n_z):
+        if s > 2:
+            mark(f"pass{s+1}")
+            if s + 1 < n_z:
+                pass_on(s + 1)
+        mark(f"send{s-1}")
+        expert_send(s - 1)
+        mark(f"fromy{s}")
         from_y(s)
-        mark(f"i_kvf{s+2}")
-        if s + 2 < n_z:
-            kv_forward(s + 2)
-        mark(f"i_in{s}")
+        mark(f"kvf{s}")
+        if s < n_z // 2:
+            kv_forward(s, outward, False)
+        if s < n_z - 1:
+            kv_forward(s, -outward, False)
+        if s == 2:
+            mark("att1x")
+            near_arrived(1)
+            attend_second(1, others)
+        if s == 3:
+            mark("att2")
+            attend_first(2, others)
+        if s == n_z - 1:
+            mark(f"kvg{s}")
+            kv_forward(s, -outward, True)
+        mark(f"in{s}")
         row_scale = expert_in(s)
-        mark(f"i_hid{s}")
+        mark(f"hid{s}")
         expert_hidden(s, row_scale)
-        mark(f"i_pass{s+1}")
-        if s + 1 < stages:
-            pass_on(s + 1)
-        mark(f"i_down{s}")
+        mark(f"down{s}")
         expert_down(s)
-        mark(f"i_ret{s-1}")
-        expert_return(s - 1)
-        mark(f"i_send{s}")
-        expert_send(s)
-
-    mark("j_farkv")
-
-    def far_attend(owner):
-        for k in range(2, n_z):
-            z = z_near(k)
-
-            def one(i, carry):
-                attend(z * n_x + (my_x + i) % n_x, owner)
-                return carry
-
-            lax.fori_loop(0, n_x, one, 0)
-
-    for k in range(2, n_z):
-        for i in range(1, n_x):
-            kv_arrived(z_near(k) * n_x + (my_x + i) % n_x)
-    mark("j_loadmix")
+        if s < n_z - 1:
+            mark(f"kvg{s}")
+            kv_forward(s, -outward, True)
+    mark("att2x")
+    near_arrived(2)
+    attend_second(2, others)
+    mark("send")
+    expert_send(n_z - 1)
+    mark("ret0")
+    expert_return(0)
+    expert_return(1)
     loads[12].wait()
+    mark("arr3")
+    for k in range(3, n_z):
+        near_arrived(k)
+    for whose in (1 - core, core):
+        if whose is core:
+            mark("ret2")
+            for o in range(2, n_z - 1):
+                expert_return(o)
+        for owner in others:
+            mark("att3")
+            for k in range(3, n_z):
+                attend_both(k, owner * piece + whose * half, half)
+            mark("mix")
+            mix(owner, whose)
+            if whose is not core:
+                mix_mate(owner, 1 - core).start()
+    mark("k_mixsum")
     for j in range(1, n_y):
-        mark("j_att")
-        far_attend(y_peer(j))
-        if j == 1:
-            mark("j_ret")
-            expert_return(stages - 1)
-        mark("j_mix")
-        mix(y_peer(j))
-    mark("k_att")
-    far_attend(my_y)
-    for j in range(1, n_y):
-        mark("k_mixsum")
         ms_out[y_peer(j)] = mix_sum(y_peer(j)).astype(BF)
-        mix_y(j, my_y).start()
+        for c in range(pieces):
+            mix_y(j, my_y, c).start()
+    mark("k_ret")
+    expert_return(n_z - 1)
+    mark("k_att2")
+
+    for k in range(1, n_z):
+        attend_both(k, my_y * piece, piece)
     mark("k_mix")
-    mix(my_y)
+    mix(my_y, 1 - core)
+    mix_mate(my_y, 1 - core).start()
+    mix(my_y, core)
 
     mark("l_retwait")
 
@@ -602,7 +656,8 @@
     total = mix_sum(my_y)
     mark("n_ywait")
     for j in range(1, n_y):
-        mix_y(j, y_peer(j)).wait_recv()
+        for c in range(pieces):
+            mix_y(j, y_peer(j), c).wait_recv()
         total = total + my_in[y_peer(j)].astype(F32)
     mark("n_out")
     mixed_ref[...] = total.astype(BF)
@@ -632,12 +687,13 @@
     def _():
         own_kv_left().wait_send()
 
-    for k in range(1, n_z):
-        inside, onward = kv_onward(k)
-
-        @pl.when(inside)
-        def _():
-            onward.wait_send()
+    for t in range(1, n_z):
+        for way in (outward, -outward):
+            there, beyond, z, onward = kv_pass(t, way)
+
+            @pl.when(jnp.logical_and(there, beyond))
+            def _():
+                onward.wait_send()
 
     for j in range(1, n_y):
 
@@ -646,13 +702,15 @@
             return carry
 
         lax.fori_loop(0, n_ep, sent_y, 0)
-        mix_y(j, my_y).wait_send()
+        for c in range(pieces):
+            mix_y(j, my_y, c).wait_send()
     for j in range(n_y):
         for s in range(stages):
             to_mate(y_peer(j), core, s).wait_send()
-            expert_mate(y_peer(j), 1 - core, s).wait_send()
+        for o in range(n_z):
+            expert_mate(y_peer(j), 1 - core, o).wait_send()
             if j:
-                expert_y(j, my_y, s).wait_send()
+                expert_y(j, my_y, o).wait_send()
         mix_mate(y_peer(j), 1 - core).wait_send()
     mark(None)
 
@@ -667,7 +725,7 @@
     n_y = n_tp // 2
     n_x = 1 << ((n_ep.bit_length() - 1) // 2)
     n_z = n_ep // n_x
-    stages = n_z - 1
+    stages = n_z
     spare = heads % 2 * HD
     if spare:
         queries = jnp.pad(queries, ((0, 0), (0, spare)))
@@ -688,7 +746,7 @@
         vm((1, HD), F32), vm((1, HD), F32), vm((1, width), F32), vm((top, tokens), jnp.int32), vm((top, tokens), F32),
         vm((width, hidden_w), BF), vm((width, hidden_w), BF), vm((hidden_w, width), BF),
         vm(mix_out_weight.shape, BF),
-        vm((n_ep, rows, LANES), BF), vm((heads, rows, LANES), BF), vm((n_y, heads * rows // n_y, LANES), F32),
+        vm((n_ep, rows, LANES), BF), vm((heads, rows, LANES), BF), vm((heads, rows, LANES), F32),
         vm((n_ep, slots_per, col_w), BF), vm((n_tp, n_ep, slots_per, col_w), BF),
         vm((slots, width), BF), vm((slots, hidden_w), BF),
         vm((n_tp, slots, col_w), BF), vm((n_y, slots, col_w), BF), vm((n_y, slots, col_w), BF),
@@ -699,20 +757,20 @@
         dma((13,)),
         dma((n_z, n_x)), dma((n_z, 2)), dma((n_ep,)), dma((n_ep,)), dma((n_ep,)),
         dma((n_y, n_ep)), dma((n_y, n_ep)),
-    ] + [dma((n_y, stages))] * 6 + [dma((n_ep,))] * 2 + [dma((n_y,))] * 4
+    ] + [dma((n_y, stages))] * 2 + [dma((n_y, n_z))] * 4 + [dma((n_ep,))] * 2 + [dma((n_y,))] * 2 + [dma((n_y, 2))] * 2
     in_vmem = pl.BlockSpec(memory_space=pltpu.VMEM)
     in_hbm = pl.BlockSpec(memory_space=pltpu.HBM)
     return pl.pallas_call(
         functools.partial(kernel, n_ep, n_tp, heads, width),
         out_shape=(
-            jax.ShapeDtypeStruct((half, out_w), BF),
-            jax.ShapeDtypeStruct((tokens, col_w), BF),
+            pltpu.VMEM((half, out_w), BF),
+            pltpu.VMEM((tokens, col_w), BF),
         ),
         in_specs=[in_hbm] * 13,
         out_specs=(in_vmem, in_vmem),
         scratch_shapes=scratch,
         compiler_params=pltpu.CompilerParams(
-            collective_id=0, has_side_effects=True, vmem_limit_bytes=60 * 1024 * 1024
+            collective_id=0, has_side_effects=True, vmem_limit_bytes=56 * 1024 * 1024
         ),
     )(
         queries, key_input, value_input, query_gain[None, :], key_gain[None, :],

time: 75 us -> 55.2 us (0.74)
  Pallas kernels: 70.7 us -> 52.9 us
  local copies, waits for them, and re-layouts: 3.47 us -> 1.46 us
    pallas_call x1, Pallas kernels: 70.7 us -> 52.9 us  [local(): pl.pallas_call(functools.partial(kernel, n_ep, n_tp, heads, width), out_s...]
    unnamed x2, local copies, waits for them, and re-layouts: 3.47 us -> 1.46 us
where the time goes in v2:
time: 55.2 us; the launch traced here: 55 us
  Pallas kernels  52.9 us (96%)
  local copies, waits for them, and re-layouts  1.46 us (3%)
  between operations  0.64 us (1%)
    pallas_call x1, Pallas kernels, local(): pl.pallas_call(functools.partial(kernel, n_ep, n_tp, heads, width), out_s...  52.9 us
    unnamed x2, local copies, waits for them, and re-layouts  1.46 us

profile of v2, /device:TPU:0, one launch (start us, length us, event | category | flops | bytes accessed | tf_op | source)
XLA Modules:
  0.0 55.0 jit_solution(12520702497048407161)
XLA Ops:
  0.6 52.9 %shard_map.140 = (bf16[128,2048]{1,0:T(8,128)(2,1)S(1)}, bf16[160,512]{1,0:T(8,128)(2,1)S(1)}) custom-call(bf16[512,256]{1,0:T(8,128)(2,1)} %q_any.1, bf16[512,256]{1,0:T(8,128)(2,1)} %k_any.1, bf16[512,256]{1,0:T(8,128)(2,1)} %v_any.1, f32[1,64]{1,0:T(1,128)} %bitcast.8, f32[1,64]{1,0:T(1,128)} %bitcast.9, bf16[256,2048]{1,0:T(8,128)(2,1)} %wmix_any.1, ...), custom_call_target="tpu_custom_call" | custom-call | tf_op jit(solution)/shard_map/pallas_call | solution.py:763
  53.6 0.8 %copy.17 = bf16[128,2048]{1,0:T(8,128)(2,1)} copy(bf16[128,2048]{1,0:T(8,128)(2,1)S(1)} %get-tuple-element.2) | data formatting | bytes 1048576
  54.4 0.7 %copy.18 = bf16[160,512]{1,0:T(8,128)(2,1)} copy(bf16[160,512]{1,0:T(8,128)(2,1)S(1)} %get-tuple-element.3) | data formatting | bytes 327680

commit v3 on v2

--- a/solution.py
+++ b/solution.py
@@ -154,6 +154,7 @@
     pl.semaphore_signal(barrier, inc=1, device_id=(me, mate), device_id_type=MESH)
 
     mark("b_route")
+    cos_table, sin_table = angle_tables(me * rows, rows)
     loads[0].wait()
     expert_row = lax.broadcasted_iota(jnp.int32, (n_ep, tokens), 0)
     first = jnp.where(expert_row == routes_ref[0:1, :], 1.0, 0.0)
@@ -222,14 +223,12 @@
 
     @pl.when(jnp.logical_not(at_end))
     def _():
-        for o in range(2, n_z):
-            dispatch(o)
+        dispatch(2)
 
     for j in range(1, n_y):
         over_y(j, me, my_y).start()
 
     mark("f_prepk")
-    cos_table, sin_table = angle_tables(me * rows, rows)
     for i in (2, 3, 4):
         loads[i].wait()
     odd = kv_head % 2 == 1
@@ -254,8 +253,10 @@
 
     @pl.when(at_end)
     def _():
-        for o in range(2, n_z):
-            dispatch(o)
+        dispatch(2)
+
+    for o in range(3, n_z):
+        dispatch(o)
 
     side = my_z // (n_z // 2)
     outward = 1 - 2 * side
@@ -507,12 +508,6 @@
     def attend_both(k, start, many):
         attend(z_near(k) * n_x, n_x, start, many)
 
-    def expert_rows(s):
-        mark(f"in{s}")
-        row_scale = expert_in(s)
-        mark(f"hid{s}")
-        expert_hidden(s, row_scale)
-
     mark("g_attown")
     attend_all(me, True)
     mark("g_pass0")
@@ -523,14 +518,18 @@
     from_y(0)
     mark("kva")
     kv_forward(1, outward, False)
-    kv_forward(1, -outward, True)
     mark("attownx")
     others_attend(my_z)
     loads[7].wait()
     loads[9].wait()
     loads[10].wait()
     loads[11].wait()
-    expert_rows(0)
+    mark("in0")
+    row_scale = expert_in(0)
+    mark("kvb")
+    kv_forward(1, -outward, True)
+    mark("hid0")
+    expert_hidden(0, row_scale)
     mark("fromy1")
     from_y(1)
     mark("pass2")
@@ -551,30 +550,32 @@
     attend_first(1, others)
     mark("send0")
     expert_send(0)
+    mark("kvf2")
+    kv_forward(2, -outward, False)
     for s in range(2, n_z):
         if s > 2:
             mark(f"pass{s+1}")
             if s + 1 < n_z:
                 pass_on(s + 1)
-        mark(f"send{s-1}")
-        expert_send(s - 1)
         mark(f"fromy{s}")
         from_y(s)
         mark(f"kvf{s}")
         if s < n_z // 2:
             kv_forward(s, outward, False)
-        if s < n_z - 1:
+        if 2 < s < n_z - 1:
             kv_forward(s, -outward, False)
         if s == 2:
             mark("att1x")
             near_arrived(1)
             attend_second(1, others)
+        if s == n_z - 1:
+            mark(f"kvg{s}")
+            kv_forward(s, -outward, True)
         if s == 3:
             mark("att2")
             attend_first(2, others)
-        if s == n_z - 1:
-            mark(f"kvg{s}")
-            kv_forward(s, -outward, True)
+        mark(f"send{s-1}")
+        expert_send(s - 1)
         mark(f"in{s}")
         row_scale = expert_in(s)
         mark(f"hid{s}")
@@ -625,6 +626,9 @@
     mix_mate(my_y, 1 - core).start()
     mix(my_y, core)
 
+    mark("n_mixsum")
+    total = mix_sum(my_y)
+
     mark("l_retwait")
 
     def ret_wait(o, carry):
@@ -652,16 +656,6 @@
     )
     out_ref[...] = (rows_a * share_a + rows_b * share_b).astype(BF)
 
-    mark("n_mixsum")
-    total = mix_sum(my_y)
-    mark("n_ywait")
-    for j in range(1, n_y):
-        for c in range(pieces):
-            mix_y(j, y_peer(j), c).wait_recv()
-        total = total + my_in[y_peer(j)].astype(F32)
-    mark("n_out")
-    mixed_ref[...] = total.astype(BF)
-
     mark("o_sends")
 
     def sends(o, carry):
@@ -702,8 +696,6 @@
             return carry
 
         lax.fori_loop(0, n_ep, sent_y, 0)
-        for c in range(pieces):
-            mix_y(j, my_y, c).wait_send()
     for j in range(n_y):
         for s in range(stages):
             to_mate(y_peer(j), core, s).wait_send()
@@ -712,6 +704,17 @@
             if j:
                 expert_y(j, my_y, o).wait_send()
         mix_mate(y_peer(j), 1 - core).wait_send()
+
+    mark("n_ywait")
+    for j in range(1, n_y):
+        for c in range(pieces):
+            mix_y(j, y_peer(j), c).wait_recv()
+        total = total + my_in[y_peer(j)].astype(F32)
+    mark("n_out")
+    mixed_ref[...] = total.astype(BF)
+    for j in range(1, n_y):
+        for c in range(pieces):
+            mix_y(j, my_y, c).wait_send()
     mark(None)
 
 

time: 55.2 us -> 53.6 us (0.971)
  Pallas kernels: 52.9 us -> 51.3 us
    pallas_call x1, Pallas kernels: 52.9 us -> 51.3 us  [local(): pl.pallas_call(functools.partial(kernel, n_ep, n_tp, heads, width), out_s...]
where the time goes in v3:
time: 53.6 us; the launch traced here: 53.4 us
  Pallas kernels  51.3 us (96%)
  local copies, waits for them, and re-layouts  1.46 us (3%)
  between operations  0.64 us (1%)
    pallas_call x1, Pallas kernels, local(): pl.pallas_call(functools.partial(kernel, n_ep, n_tp, heads, width), out_s...  51.3 us
    unnamed x2, local copies, waits for them, and re-layouts  1.46 us

profile of v3, /device:TPU:0, one launch (start us, length us, event | category | flops | bytes accessed | tf_op | source)
XLA Modules:
  0.0 53.4 jit_solution(8317666260424591122)
XLA Ops:
  0.6 51.3 %shard_map.140 = (bf16[128,2048]{1,0:T(8,128)(2,1)S(1)}, bf16[160,512]{1,0:T(8,128)(2,1)S(1)}) custom-call(bf16[512,256]{1,0:T(8,128)(2,1)} %q_any.1, bf16[512,256]{1,0:T(8,128)(2,1)} %k_any.1, bf16[512,256]{1,0:T(8,128)(2,1)} %v_any.1, f32[1,64]{1,0:T(1,128)} %bitcast.8, f32[1,64]{1,0:T(1,128)} %bitcast.9, bf16[256,2048]{1,0:T(8,128)(2,1)} %wmix_any.1, ...), custom_call_target="tpu_custom_call" | custom-call | tf_op jit(solution)/shard_map/pallas_call | solution.py:766
  51.9 0.8 %copy.17 = bf16[128,2048]{1,0:T(8,128)(2,1)} copy(bf16[128,2048]{1,0:T(8,128)(2,1)S(1)} %get-tuple-element.2) | data formatting | bytes 1048576
  52.7 0.7 %copy.18 = bf16[160,512]{1,0:T(8,128)(2,1)} copy(bf16[160,512]{1,0:T(8,128)(2,1)S(1)} %get-tuple-element.3) | data formatting | bytes 327680
